TPU v7x, 512 devices: a whole 4x4x16 slice. The times are simulated.
512 devices in a mesh: ep: 16 (over y, x), tp: 32 (over z, core).
Axes of the slice: x: 4, y: 4, z: 16, core: 2. Of those that a mesh axis runs over, the one named last changes fastest.
Arguments:
- tokens: bfloat16 [4096, 2048], P('ep', 'tp'), may hold values from -600 to 600
- pre_gain: float32 [2048], P('tp'), may hold values from 0.1 to 1.9
- expert_gate: bfloat16 [16, 2048, 8192], P('ep', None, 'tp'), may hold values from -0.125 to 0.125
- expert_up: bfloat16 [16, 2048, 8192], P('ep', None, 'tp'), may hold values from -0.125 to 0.125
- expert_down: bfloat16 [16, 8192, 2048], P('ep', 'tp'), may hold values from -8 to 8
- routes: int32 [4096, 2], P('ep'), may hold values from 0 to 15, all different within a row; in each aligned block of 256 rows (0 to 255, 256 to 511, ...) at most 48 rows name the same one
- route_weights: float32 [4096, 2], P('ep'), may hold values from 0.1 to 1
- post_gain: float32 [2048], P('tp'), may hold values from 0.1 to 1.9
Outputs:
- layer_out: bfloat16 [4096, 2048], P('ep', 'tp')
Inputs may be any that keep to these rules, and one draw needn't show every extreme that they name: `routes`: each token names 2 different experts. Among the 256 tokens of one index of ep no expert is named more than 48 times, a bound that some expert reaches in some of these blocks.
All inputs are finite; a program needn't handle non-finite values.
Results may differ from a plain program's by a relative error of at most 0.024.
Values may be sent and summed in bfloat16 or wider, within the bound.
No kernel may reach another device: no remote copies, remote signals or barrier semaphores. Data moves between devices by JAX's collectives and lax.ppermute only.
A program may use at most 64 MiB of HBM per device.

v0:
```python
import jax
import jax.numpy as jnp
from jax import lax
from jax.sharding import Mesh
from jax.sharding import PartitionSpec as P

TP = ("tp_0", "tp_1")
EPSILON = 1e-06


def sent_to_all(value, axis):
    copies = jnp.broadcast_to(value, (lax.axis_size(axis), *value.shape))
    return lax.all_to_all(copies, axis, split_axis=0, concat_axis=0, tiled=True)


def taken_together(value, axis):
    everything = sent_to_all(value, axis)
    return jnp.sum(everything, axis=0)


def own_block(parts, axes, turns):
    lengths = [lax.axis_size(a) for a in axes]
    parts = parts.reshape(*lengths, *parts.shape[1:])
    parts = parts.transpose(*turns, *range(len(axes), parts.ndim))
    parts = parts.reshape(-1, *parts.shape[len(axes) :])
    for k in turns:
        parts = lax.psum_scatter(parts, axes[k], scatter_dimension=0, tiled=True)
    return parts[0]


def split_up(value, dim, peers):
    before, after = (value.shape[:dim], value.shape[dim + 1 :])
    return jnp.moveaxis(value.reshape(*before, peers, -1, *after), dim, 0)


def summed_rows(value, axes, turns, dim):
    peers = lax.axis_size(axes)
    return own_block(split_up(value, dim, peers), axes, turns)


def local(tokens, pre_gain, expert_gate, expert_up, expert_down, routes, route_weights, post_gain):
    local_experts = expert_gate.shape[0]
    groups = lax.axis_size("ep")
    experts_all = local_experts * groups
    tok_rows, part_width = tokens.shape
    full_width = part_width * lax.axis_size(TP)
    capacity = 3 * tok_rows // experts_all
    values = tokens.astype(jnp.float32)
    input_sq = taken_together(jnp.sum(values * values, axis=-1), TP)
    normed = (
        values * lax.rsqrt(input_sq / full_width + EPSILON)[:, None] * pre_gain[None, :]
    ).astype(jnp.bfloat16)
    onehot = (routes[:, :, None] == jnp.arange(experts_all, dtype=jnp.int32)).astype(jnp.int32)
    onehot = onehot.reshape(tok_rows * 2, experts_all)
    earlier = jnp.cumsum(onehot, axis=0) - onehot
    slots = jnp.sum(earlier * onehot, axis=-1).reshape(tok_rows, 2)
    positions = routes * capacity + slots
    places = jnp.arange(experts_all * capacity, dtype=jnp.int32)
    first_pick = (places[:, None] == positions[None, :, 0]).astype(jnp.bfloat16)
    second_pick = (places[:, None] == positions[None, :, 1]).astype(jnp.bfloat16)
    dispatch = first_pick + second_pick
    outgoing = jnp.dot(dispatch, normed, preferred_element_type=jnp.float32).astype(jnp.bfloat16)
    arrived = lax.all_to_all(outgoing, "ep", split_axis=0, concat_axis=0, tiled=True)
    fragment = lax.all_gather(arrived, TP, axis=1, tiled=True)
    count = fragment.shape[1]
    grouped = fragment.reshape(groups, local_experts, capacity, count)
    gate_pre = jnp.einsum(
        "secw,ewf->secf", grouped, expert_gate, preferred_element_type=jnp.float32
    )
    up_pre = jnp.einsum("secw,ewf->secf", grouped, expert_up, preferred_element_type=jnp.float32)
    hidden = (jax.nn.silu(gate_pre) * up_pre).astype(jnp.bfloat16)
    product = jnp.einsum("secf,efd->dsec", hidden, expert_down, preferred_element_type=jnp.float32)
    summed = summed_rows(
        product.reshape(part_width * lax.axis_size(TP), groups * local_experts * capacity).astype(
            jnp.bfloat16
        ),
        TP,
        (1, 0),
        0,
    ).astype(jnp.float32)
    expert_out = summed.astype(jnp.bfloat16)
    returned = lax.all_to_all(expert_out, "ep", split_axis=1, concat_axis=1, tiled=True)
    contract = (((0,), (1,)), ((), ()))
    first_out = lax.dot_general(first_pick, returned, contract, preferred_element_type=jnp.float32)
    second_out = lax.dot_general(
        second_pick, returned, contract, preferred_element_type=jnp.float32
    )
    combined = route_weights[:, 0:1] * first_out + route_weights[:, 1:2] * second_out
    output_sq = taken_together(jnp.sum(combined * combined, axis=-1), TP)
    scaled = combined * lax.rsqrt(output_sq / full_width + EPSILON)[:, None] * post_gain[None, :]
    return scaled.astype(jnp.bfloat16)


def solution(mesh):
    torus = Mesh(mesh.devices.reshape(mesh.shape["ep"], 16, 2), ("ep", "tp_0", "tp_1"))
    in_specs = (
        P("ep", TP),
        P(TP),
        P("ep", None, TP),
        P("ep", None, TP),
        P("ep", TP, None),
        P("ep", None),
        P("ep", None),
        P(TP),
    )
    out_specs = P("ep", TP)
    return jax.shard_map(local, mesh=torus, in_specs=in_specs, out_specs=out_specs, check_vma=False)
```

profile of v0, /device:TPU:1, one launch (start us, length us, event | category | flops | bytes accessed | tf_op | source)
XLA Modules:
  0.0 277.1 jit_solution(4352224880434988949)
XLA Ops:
  6.5 0.9 fusion.16
  7.4 0.6 broadcast_in_dim.4
  8.0 16.7 %all-to-all-start = ((f32[32,1,256]{2,1,0:T(1,128)}), f32[32,1,256]{2,1,0:T(1,128)S(1)}, u32[]{:S(2)}, u32[]{:S(2)}) async-start(f32[32,1,256]{2,1,0:T(1,128)} %broadcast_in_dim.4), calls=%async_computation | async-start | bytes 65536 | tf_op jit(solution)/shard_map/all_to_all | solution.py:13
  24.8 0.8 copy.64
  26.0 1.2 reduce-window.6
  27.1 0.2 slice_reduce_fusion
  27.7 0.7 multiply_add_fusion
  28.4 8.4 %all-to-all-done = f32[32,1,256]{2,1,0:T(1,128)S(1)} async-done(((f32[32,1,256]{2,1,0:T(1,128)}), f32[32,1,256]{2,1,0:T(1,128)S(1)}, u32[]{:S(2)}, u32[]{:S(2)}) %all-to-all-start) | async-done | bytes 32800 | tf_op jit(solution)/shard_map/all_to_all | solution.py:13
  36.9 1.1 convolution_convert_fusion.1
  38.0 0.2 copy.77
  38.2 0.2 reshape.84
  38.3 13.2 %all_to_all.36 = bf16[16,2,1536]{2,1,0:T(2,128)(2,1)S(1)} all-to-all(bf16[16,2,1536]{2,1,0:T(2,128)(2,1)S(1)} %reshape.84), channel_id=1, replica_groups=mesh['ep'=16,'tp_0'=16,'tp_1'=2] {'ep'}, dimensions={0} | all-to-all | bytes 196608 | tf_op jit(solution)/shard_map/all_to_all | solution.py:63
  51.5 0.2 reshape.85
  51.7 0.8 copy.78
  52.6 63.2 %all-gather.2.cloned.1.call-done = bf16[768,2048]{0,1:T(8,128)(2,1)} async-done(((bf16[768,64]{0,1:T(8,128)(2,1)}), bf16[768,2048]{0,1:T(8,128)(2,1)}) %all-gather.2.cloned.1.call-update) | async-done | bytes 3145744 | tf_op jit(solution)/shard_map/all_gather | solution.py:64
  115.7 4.7 %copy.71 = bf16[768,2048]{1,0:T(8,128)(2,1)} copy(bf16[768,2048]{0,1:T(8,128)(2,1)} %all-gather.2.cloned.1.call-done) | data formatting | bytes 6291456 | tf_op jit(solution)/shard_map/all_gather | solution.py:64
  120.4 3.0 %convolution_bitcast_fusion.1 = f32[16,1,48,256]{3,2,0,1:T(8,128)S(1)} fusion(bf16[16,48,2048]{2,1,0:T(8,128)(2,1)} %bitcast.71, bf16[1,2048,256]{2,1,0:T(8,128)(2,1)S(1)} %copy-done.4), kind=kOutput, calls=%fused_computation.3 | convolution fusion | flops 805306368 | bytes 4980736 | tf_op jit(solution)/shard_map/secw,ewf->secf/dot_general | solution.py:67
  123.6 1.0 fusion.2
  124.6 2.7 fusion
  127.3 4.6 %copy.72 = bf16[2048,768]{1,0:T(8,128)(2,1)} copy(bf16[2048,768]{0,1:T(8,128)(2,1)} %fusion) | data formatting | bytes 6291456 | tf_op jit(solution)/shard_map/convert_element_type | solution.py:74
  131.9 3.9 %copy.73 = bf16[2,16,64,768]{3,2,1,0:T(8,128)(2,1)} copy(bf16[2,16,64,768]{3,2,0,1:T(8,128)(2,1)} %bitcast.70) | data formatting | bytes 6291456 | tf_op jit(solution)/shard_map/transpose | solution.py:24
  135.9 18.9 %reduce-scatter.3.cloned.1.call-done = bf16[16,64,768]{2,1,0:T(8,128)(2,1)} async-done(((bf16[32,64,768]{2,1,0:T(8,128)(2,1)}), bf16[16,64,768]{2,1,0:T(8,128)(2,1)}) %reduce-scatter.3.cloned.1.call-update) | async-done | bytes 1572880 | tf_op jit(solution)/shard_map/reduce_scatter | solution.py:27
  154.8 66.2 %reduce-scatter.5.cloned.1.call-done = bf16[1,64,768]{2,1,0:T(8,128)(2,1)} async-done(((bf16[16,64,768]{2,1,0:T(8,128)(2,1)}), bf16[1,64,768]{2,1,0:T(8,128)(2,1)}) %reduce-scatter.5.cloned.1.call-update) | async-done | bytes 98320 | tf_op jit(solution)/shard_map/reduce_scatter | solution.py:27
  221.0 1.1 copy.79
  222.1 0.8 reshape.86
  222.9 6.4 %all-to-all-start.2 = ((bf16[16,2,1536]{2,1,0:T(2,128)(2,1)}), bf16[16,2,1536]{2,1,0:T(2,128)(2,1)S(1)}, u32[]{:S(2)}, u32[]{:S(2)}) async-start(bf16[16,2,1536]{2,1,0:T(2,128)(2,1)} %reshape.86), calls=%async_computation.4 | async-start | bytes 196608 | tf_op jit(solution)/shard_map/all_to_all | solution.py:82
  229.4 6.6 %all-to-all-done.2 = bf16[16,2,1536]{2,1,0:T(2,128)(2,1)S(1)} async-done(((bf16[16,2,1536]{2,1,0:T(2,128)(2,1)}), bf16[16,2,1536]{2,1,0:T(2,128)(2,1)S(1)}, u32[]{:S(2)}, u32[]{:S(2)}) %all-to-all-start.2) | async-done | bytes 98336 | tf_op jit(solution)/shard_map/all_to_all | solution.py:82
  236.0 0.2 reshape.87
  236.2 0.3 convolution_multiply_fusion.1
  236.5 0.3 multiply_reduce_fusion
  236.8 33.0 %all_to_all.37 = f32[32,1,256]{2,1,0:T(1,128)S(1)} all-to-all(f32[32,1,256]{2,1,0:T(1,128)S(1)} %broadcast_in_dim.5), channel_id=1, replica_groups=mesh['ep'=16,'tp_0'=16,'tp_1'=2] {'tp_0','tp_1'}, dimensions={0} | all-to-all | bytes 65536 | tf_op jit(solution)/shard_map/all_to_all | solution.py:13
  269.9 0.7 multiply_convert_fusion
  (33 shorter events, 1.1 us)
Async XLA Ops:
  6.5 118.0 %copy-start = (bf16[1,256,2048]{2,1,0:T(8,128)(2,1)S(1)}, bf16[1,256,2048]{2,1,0:T(8,128)(2,1)}, u32[]{:S(2)}) copy-start(bf16[1,256,2048]{2,1,0:T(8,128)(2,1)} %param.12) | copy-start | bytes 3145732
  8.0 28.8 %all-to-all-start = ((f32[32,1,256]{2,1,0:T(1,128)}), f32[32,1,256]{2,1,0:T(1,128)S(1)}, u32[]{:S(2)}, u32[]{:S(2)}) async-start(f32[32,1,256]{2,1,0:T(1,128)} %broadcast_in_dim.4), calls=%async_computation | async-start | bytes 65536 | tf_op jit(solution)/shard_map/all_to_all | solution.py:13
  24.8 90.9 %all-gather.2.cloned.1.call-start = ((), (), s32[]{:S(2)}) async-start(), calls=%async_computation.6 | async-start | bytes 3244032 | tf_op jit(solution)/shard_map/all_gather | solution.py:64
  52.5 67.9 %copy-start.4 = (bf16[1,2048,256]{2,1,0:T(8,128)(2,1)S(1)}, bf16[1,2048,256]{2,1,0:T(8,128)(2,1)}, u32[]{:S(2)}) copy-start(bf16[1,2048,256]{2,1,0:T(8,128)(2,1)} %param.10) | copy-start | bytes 3145732
  52.5 102.3 %reduce-scatter.3.cloned.1.call-start = ((), (), s32[]{:S(2)}) async-start(), calls=%async_computation.7 | async-start | bytes 4718592 | tf_op jit(solution)/shard_map/reduce_scatter | solution.py:27
  120.4 3.1 %copy-start.1 = (bf16[768,2048]{1,0:T(8,128)(2,1)S(1)}, bf16[768,2048]{1,0:T(8,128)(2,1)}, u32[]{:S(2)}) copy-start(bf16[768,2048]{1,0:T(8,128)(2,1)} %copy.71) | copy-start | bytes 9437188
  120.4 3.1 %copy-start.5 = (bf16[1,2048,256]{2,1,0:T(8,128)(2,1)S(1)}, bf16[1,2048,256]{2,1,0:T(8,128)(2,1)}, u32[]{:S(2)}) copy-start(bf16[1,2048,256]{2,1,0:T(8,128)(2,1)} %param.11) | copy-start | bytes 3145732
  135.8 93.5 %copy-start.2 = (f32[256,2]{0,1:T(2,128)S(1)}, f32[256,2]{0,1:T(2,128)}, u32[]{:S(2)}) copy-start(f32[256,2]{0,1:T(2,128)} %param.14) | copy-start | bytes 6148
  135.8 134.0 %copy-start.3 = (f32[64]{0:T(128)S(1)}, f32[64]{0:T(128)}, u32[]{:S(2)}) copy-start(f32[64]{0:T(128)} %param.15) | copy-start | bytes 772
  135.9 85.2 %reduce-scatter.5.cloned.1.call-start = ((), (), s32[]{:S(2)}) async-start(), calls=%async_computation.8 | async-start | bytes 1671168 | tf_op jit(solution)/shard_map/reduce_scatter | solution.py:27
  222.9 13.1 %all-to-all-start.2 = ((bf16[16,2,1536]{2,1,0:T(2,128)(2,1)}), bf16[16,2,1536]{2,1,0:T(2,128)(2,1)S(1)}, u32[]{:S(2)}, u32[]{:S(2)}) async-start(bf16[16,2,1536]{2,1,0:T(2,128)(2,1)} %reshape.86), calls=%async_computation.4 | async-start | bytes 196608 | tf_op jit(solution)/shard_map/all_to_all | solution.py:82
Sparse Core Ops, SparseCore 0:
  52.6 63.0 all-gather.1
  136.0 18.7 reduce-scatter.2
  157.6 63.3 reduce-scatter.4
where the time goes:
time: 278 us; the launch traced here: 277 us
  waiting for transfers between devices  163 us (59%)
  blocking collectives  46.2 us (17%)
  starting transfers between devices  23.3 us (8%)
  local copies, waits for them, and re-layouts  18.8 us (7%)
  between operations  13.3 us (5%)
  matrix products  8.38 us (3%)
  other arithmetic  3.68 us (1%)
    reduce_scatter x2, waiting for transfers between devices, own_block(): parts = lax.psum_scatter(parts, axes[k], scatter_dimension=0, tiled=True)  85.1 us
    all_gather x1, waiting for transfers between devices, local(): fragment = lax.all_gather(arrived, TP, axis=1, tiled=True)  63.2 us
    all_to_all x1, blocking collectives, sent_to_all(): return lax.all_to_all(copies, axis, split_axis=0, concat_axis=0, tiled=True)  33 us
    all_to_all x1, starting transfers between devices, sent_to_all(): return lax.all_to_all(copies, axis, split_axis=0, concat_axis=0, tiled=True)  16.7 us
    all_to_all x1, blocking collectives, local(): lax.all_to_all(outgoing, 'ep', split_axis=0, concat_axis=0, tiled=True)  13.2 us
    all_to_all x1, waiting for transfers between devices, sent_to_all(): return lax.all_to_all(copies, axis, split_axis=0, concat_axis=0, tiled=True)  8.44 us
    all_to_all x1, waiting for transfers between devices, local(): lax.all_to_all(expert_out, 'ep', split_axis=1, concat_axis=1, tiled=True)  6.64 us
    all_to_all x1, starting transfers between devices, local(): lax.all_to_all(expert_out, 'ep', split_axis=1, concat_axis=1, tiled=True)  6.45 us
  transfers between devices with their start and end apart: 5, of which 5 were waited for; matrix products, arithmetic and copies ran while one was open for 1% of the time, Pallas kernels for 0%

commit v1 on v0

--- a/solution.py
+++ b/solution.py
@@ -61,7 +61,9 @@
     dispatch = first_pick + second_pick
     outgoing = jnp.dot(dispatch, normed, preferred_element_type=jnp.float32).astype(jnp.bfloat16)
     arrived = lax.all_to_all(outgoing, "ep", split_axis=0, concat_axis=0, tiled=True)
-    fragment = lax.all_gather(arrived, TP, axis=1, tiled=True)
+    fragment = jnp.concatenate(
+        lax.all_to_all(jnp.stack([arrived] * lax.axis_size(TP)), TP, 0, 0), axis=1
+    )
     count = fragment.shape[1]
     grouped = fragment.reshape(groups, local_experts, capacity, count)
     gate_pre = jnp.einsum(

time: 278 us -> 373 us (1.34)
  blocking collectives: 46.2 us -> 198 us
  waiting for transfers between devices: 163 us -> 91.4 us
  local copies, waits for them, and re-layouts: 18.8 us -> 33.9 us
    all_to_all x0 -> x1, blocking collectives: none -> 152 us  [local(): lax.all_to_all(jnp.stack([arrived] * lax.axis_size(TP)), TP, 0, 0)]
    all_gather x1 -> x0, waiting for transfers between devices: 63.2 us -> none  [local(): fragment = lax.all_gather(arrived, TP, axis=1, tiled=True)]
    another operation x1 -> x4, local copies, waits for them, and re-layouts: 0.01 us -> 10.3 us
    reshape x0 -> x1, local copies, waits for them, and re-layouts: none -> 10.2 us  [local(): jnp.concatenate(lax.all_to_all(jnp.stack([arrived] * lax.axis_size(TP)),...]
    reduce_scatter x2, waiting for transfers between devices: 85.1 us -> 76.2 us  [own_block(): parts = lax.psum_scatter(parts, axes[k], scatter_dimension=0, tiled=True)]
    all_gather x1 -> x0, local copies, waits for them, and re-layouts: 4.71 us -> none  [local(): fragment = lax.all_gather(arrived, TP, axis=1, tiled=True)]
  transfers between devices with their start and end apart: 5 -> 4, of which waited for: 5 -> 4; matrix products, arithmetic and copies ran while one was open for 1% -> 1% of each run, Pallas kernels for 0% -> 0%
where the time goes in v1:
time: 373 us; the launch traced here: 372 us
  blocking collectives  198 us (53%)
  waiting for transfers between devices  91.4 us (25%)
  local copies, waits for them, and re-layouts  33.9 us (9%)
  starting transfers between devices  23.4 us (6%)
  between operations  13.6 us (4%)
  matrix products  8.38 us (2%)
    all_to_all x1, blocking collectives, local(): lax.all_to_all(jnp.stack([arrived] * lax.axis_size(TP)), TP, 0, 0)  152 us
    reduce_scatter x2, waiting for transfers between devices, own_block(): parts = lax.psum_scatter(parts, axes[k], scatter_dimension=0, tiled=True)  76.2 us
    all_to_all x1, blocking collectives, sent_to_all(): return lax.all_to_all(copies, axis, split_axis=0, concat_axis=0, tiled=True)  33 us
    all_to_all x1, starting transfers between devices, sent_to_all(): return lax.all_to_all(copies, axis, split_axis=0, concat_axis=0, tiled=True)  16.7 us
    all_to_all x1, blocking collectives, local(): lax.all_to_all(outgoing, 'ep', split_axis=0, concat_axis=0, tiled=True)  13.2 us
    reshape x1, local copies, waits for them, and re-layouts, local(): jnp.concatenate(lax.all_to_all(jnp.stack([arrived] * lax.axis_size(TP)),...  10.2 us
    another operation x2, local copies, waits for them, and re-layouts  9.83 us
    all_to_all x1, waiting for transfers between devices, sent_to_all(): return lax.all_to_all(copies, axis, split_axis=0, concat_axis=0, tiled=True)  8.44 us
  transfers between devices with their start and end apart: 4, of which 4 were waited for; matrix products, arithmetic and copies ran while one was open for 1% of the time, Pallas kernels for 0%

profile of v1, /device:TPU:1, one launch (start us, length us, event | category | flops | bytes accessed | tf_op | source)
XLA Modules:
  0.0 372.1 jit_solution(16903937679126898855)
XLA Ops:
  6.5 0.9 fusion.16
  7.4 0.6 broadcast_in_dim.4
  8.0 16.7 %all-to-all-start = ((f32[32,1,256]{2,1,0:T(1,128)}), f32[32,1,256]{2,1,0:T(1,128)S(1)}, u32[]{:S(2)}, u32[]{:S(2)}) async-start(f32[32,1,256]{2,1,0:T(1,128)} %broadcast_in_dim.4), calls=%async_computation | async-start | bytes 65536 | tf_op jit(solution)/shard_map/all_to_all | solution.py:13
  24.8 0.8 copy.64
  26.0 1.2 reduce-window.6
  27.1 0.2 slice_reduce_fusion
  27.7 0.7 multiply_add_fusion
  28.4 8.4 %all-to-all-done = f32[32,1,256]{2,1,0:T(1,128)S(1)} async-done(((f32[32,1,256]{2,1,0:T(1,128)}), f32[32,1,256]{2,1,0:T(1,128)S(1)}, u32[]{:S(2)}, u32[]{:S(2)}) %all-to-all-start) | async-done | bytes 32800 | tf_op jit(solution)/shard_map/all_to_all | solution.py:13
  36.9 1.1 convolution_convert_fusion.1
  38.0 0.2 copy.77
  38.2 0.2 reshape.90
  38.3 13.2 %all_to_all.38 = bf16[16,2,1536]{2,1,0:T(2,128)(2,1)S(1)} all-to-all(bf16[16,2,1536]{2,1,0:T(2,128)(2,1)S(1)} %reshape.90), channel_id=1, replica_groups=mesh['ep'=16,'tp_0'=16,'tp_1'=2] {'ep'}, dimensions={0} | all-to-all | bytes 196608 | tf_op jit(solution)/shard_map/all_to_all | solution.py:63
  51.9 0.3 stack.5
  52.2 151.6 %all_to_all.39 = bf16[32,768,64]{1,2,0:T(8,128)(2,1)} all-to-all(bf16[32,768,64]{1,2,0:T(8,128)(2,1)S(1)} %stack.5), channel_id=1, replica_groups=mesh['ep'=16,'tp_0'=16,'tp_1'=2] {'tp_0','tp_1'}, dimensions={0} | all-to-all | bytes 6291456 | tf_op jit(solution)/shard_map/all_to_all | solution.py:65
  203.8 10.2 %copy.71 = bf16[768,32,64]{2,1,0:T(8,128)(2,1)} copy(bf16[768,32,64]{0,2,1:T(8,128)(2,1)} %bitcast.71) | data formatting | bytes 6291456 | tf_op jit(solution)/shard_map/reshape | solution.py:64
  214.0 9.8 %reshape.82 = bf16[16,48,2048]{2,1,0:T(8,128)(2,1)} reshape(bf16[768,32,64]{2,1,0:T(8,128)(2,1)} %copy.71) | data formatting | bytes 6291456 | tf_op jit(solution)/shard_map/reshape.9
  223.8 3.0 convolution_bitcast_fusion.1
  227.0 1.0 fusion.2
  228.0 2.7 fusion
  230.7 4.6 %copy.72 = bf16[2048,768]{1,0:T(8,128)(2,1)} copy(bf16[2048,768]{0,1:T(8,128)(2,1)} %fusion) | data formatting | bytes 6291456 | tf_op jit(solution)/shard_map/convert_element_type | solution.py:76
  235.3 3.9 %copy.73 = bf16[2,16,64,768]{3,2,1,0:T(8,128)(2,1)} copy(bf16[2,16,64,768]{3,2,0,1:T(8,128)(2,1)} %bitcast.70) | data formatting | bytes 6291456 | tf_op jit(solution)/shard_map/transpose | solution.py:24
  239.3 10.2 %reduce-scatter.3.cloned.1.call-done = bf16[16,64,768]{2,1,0:T(8,128)(2,1)} async-done(((bf16[32,64,768]{2,1,0:T(8,128)(2,1)}), bf16[16,64,768]{2,1,0:T(8,128)(2,1)}) %reduce-scatter.3.cloned.1.call-update) | async-done | bytes 1572880 | tf_op jit(solution)/shard_map/reduce_scatter | solution.py:27
  249.5 66.0 %reduce-scatter.5.cloned.1.call-done = bf16[1,64,768]{2,1,0:T(8,128)(2,1)} async-done(((bf16[16,64,768]{2,1,0:T(8,128)(2,1)}), bf16[1,64,768]{2,1,0:T(8,128)(2,1)}) %reduce-scatter.5.cloned.1.call-update) | async-done | bytes 98320 | tf_op jit(solution)/shard_map/reduce_scatter | solution.py:27
  315.6 1.1 copy.79
  316.6 0.8 reshape.92
  317.4 6.6 %all-to-all-start.3 = ((bf16[16,2,1536]{2,1,0:T(2,128)(2,1)}), bf16[16,2,1536]{2,1,0:T(2,128)(2,1)S(1)}, u32[]{:S(2)}, u32[]{:S(2)}) async-start(bf16[16,2,1536]{2,1,0:T(2,128)(2,1)} %reshape.92), calls=%async_computation.5 | async-start | bytes 196608 | tf_op jit(solution)/shard_map/all_to_all | solution.py:84
  324.0 6.6 %all-to-all-done.3 = bf16[16,2,1536]{2,1,0:T(2,128)(2,1)S(1)} async-done(((bf16[16,2,1536]{2,1,0:T(2,128)(2,1)}), bf16[16,2,1536]{2,1,0:T(2,128)(2,1)S(1)}, u32[]{:S(2)}, u32[]{:S(2)}) %all-to-all-start.3) | async-done | bytes 98336 | tf_op jit(solution)/shard_map/all_to_all | solution.py:84
  330.7 0.2 reshape.93
  330.8 0.3 convolution_multiply_fusion.1
  331.1 0.3 multiply_reduce_fusion
  331.5 33.0 %all_to_all.40 = f32[32,1,256]{2,1,0:T(1,128)S(1)} all-to-all(f32[32,1,256]{2,1,0:T(1,128)S(1)} %broadcast_in_dim.5), channel_id=1, replica_groups=mesh['ep'=16,'tp_0'=16,'tp_1'=2] {'tp_0','tp_1'}, dimensions={0} | all-to-all | bytes 65536 | tf_op jit(solution)/shard_map/all_to_all | solution.py:13
  364.6 0.7 multiply_convert_fusion
  (33 shorter events, 1.3 us)
Async XLA Ops:
  6.5 221.4 %copy-start = (bf16[1,256,2048]{2,1,0:T(8,128)(2,1)S(1)}, bf16[1,256,2048]{2,1,0:T(8,128)(2,1)}, u32[]{:S(2)}) copy-start(bf16[1,256,2048]{2,1,0:T(8,128)(2,1)} %param.12) | copy-start | bytes 3145732
  8.0 28.8 %all-to-all-start = ((f32[32,1,256]{2,1,0:T(1,128)}), f32[32,1,256]{2,1,0:T(1,128)S(1)}, u32[]{:S(2)}, u32[]{:S(2)}) async-start(f32[32,1,256]{2,1,0:T(1,128)} %broadcast_in_dim.4), calls=%async_computation | async-start | bytes 65536 | tf_op jit(solution)/shard_map/all_to_all | solution.py:13
  24.8 224.7 %reduce-scatter.3.cloned.1.call-start = ((), (), s32[]{:S(2)}) async-start(), calls=%async_computation.7 | async-start | bytes 4718592 | tf_op jit(solution)/shard_map/reduce_scatter | solution.py:27
  214.0 9.8 %copy-start.4 = (bf16[1,2048,256]{2,1,0:T(8,128)(2,1)S(1)}, bf16[1,2048,256]{2,1,0:T(8,128)(2,1)}, u32[]{:S(2)}) copy-start(bf16[1,2048,256]{2,1,0:T(8,128)(2,1)} %param.10) | copy-start | bytes 3145732
  223.8 3.1 copy-start.1
  223.8 3.1 copy-start.5
  239.2 84.8 %copy-start.2 = (f32[256,2]{0,1:T(2,128)S(1)}, f32[256,2]{0,1:T(2,128)}, u32[]{:S(2)}) copy-start(f32[256,2]{0,1:T(2,128)} %param.14) | copy-start | bytes 6148
  239.2 125.3 %copy-start.3 = (f32[64]{0:T(128)S(1)}, f32[64]{0:T(128)}, u32[]{:S(2)}) copy-start(f32[64]{0:T(128)} %param.15) | copy-start | bytes 772
  239.3 76.3 %reduce-scatter.5.cloned.1.call-start = ((), (), s32[]{:S(2)}) async-start(), calls=%async_computation.8 | async-start | bytes 1671168 | tf_op jit(solution)/shard_map/reduce_scatter | solution.py:27
  317.4 13.2 %all-to-all-start.3 = ((bf16[16,2,1536]{2,1,0:T(2,128)(2,1)}), bf16[16,2,1536]{2,1,0:T(2,128)(2,1)S(1)}, u32[]{:S(2)}, u32[]{:S(2)}) async-start(bf16[16,2,1536]{2,1,0:T(2,128)(2,1)} %reshape.92), calls=%async_computation.5 | async-start | bytes 196608 | tf_op jit(solution)/shard_map/all_to_all | solution.py:84
Sparse Core Ops, SparseCore 0:
  239.4 10.0 reduce-scatter.2
  252.3 63.1 reduce-scatter.4
